TPU v7x, 32 devices: a whole 2x2x4 slice. The times are simulated.
32 devices in a mesh: sp: 4 (over z), tp: 4 (over y, x), dp: 2 (over core).
Axes of the slice: x: 2, y: 2, z: 4, core: 2. Of those that a mesh axis runs over, the one named last changes fastest.
Arguments:
- latent: bfloat16 [2, 1024, 2048], P('dp', ('sp', 'tp')), may hold values from -6 to 6
- condition: bfloat16 [2, 2048], P('dp', ('sp', 'tp')), may hold values from -6 to 6
- context: bfloat16 [2, 32, 2048], P('dp', 'sp'), may hold values from -6 to 6
- context_vector: bfloat16 [2048], P(('sp', 'tp')), may hold values from -6 to 6
- modulator: bfloat16 [2048, 6144], P(('sp', 'tp')), may hold values from -0.3125 to 0.3125
- norm_gain: float32 [2048], replicated, may hold values from 0.1 to 1.9
- query_weight: bfloat16 [2048, 512], P(None, 'tp'), may hold values from -4 to 4
- key_weight: bfloat16 [2048, 512], P(None, 'tp'), may hold values from -0.125 to 0.125
- value_weight: bfloat16 [2048, 512], P(None, 'tp'), may hold values from -0.125 to 0.125
- head_gain: float32 [128], replicated, may hold values from 0.1 to 1.9
- lambdas: float32 [4], P('tp'), may hold values from 0.3 to 0.8
- context_bias: float32 [4, 2], P('tp'), may hold values from 1.3 to 2.7
- out_weight: bfloat16 [512, 2048], P('tp'), may hold values from -0.25 to 0.25
Outputs:
- updated: bfloat16 [2, 1024, 2048], P('dp', ('sp', 'tp'))
All inputs are finite; a program needn't handle non-finite values.
Results may differ from a plain program's by a relative error of at most 0.024.
Values may be sent and summed in bfloat16 or wider, within the bound.
A program may use at most 64 MiB of HBM per device.

v0:
```python
import jax
import jax.numpy as jnp
from jax import lax
from jax.sharding import PartitionSpec as P

EPSILON = 1e-06
OUT_SCALE = 0.8
KEY_BLOCK = 2048
LOW_START = -1e30


def modulate(inputs, gain_vector, shift_vector, scale_vector):
    as_float = inputs.astype(jnp.float32)
    normed = as_float * lax.rsqrt(jnp.mean(as_float * as_float, axis=-1, keepdims=True) + EPSILON)
    return (normed * gain_vector * (1.0 + scale_vector) + shift_vector).astype(jnp.bfloat16)


def fold_block(running, queries, keys_in, values_in, key_flags, bias_table, score_scale):
    run_max, run_total, summed = running
    scores = (
        jnp.einsum("qhmd,khmd->hmqk", queries, keys_in, preferred_element_type=jnp.float32)
        * score_scale
    )
    if key_flags is not None:
        scores = scores + bias_table[:, :, None, None] * key_flags
    new_max = jnp.maximum(run_max, jnp.max(scores, axis=-1))
    shrink = jnp.exp(run_max - new_max)
    weights = jnp.exp(scores - new_max[..., None])
    run_total = run_total * shrink + jnp.sum(weights, axis=-1)
    summed = summed * shrink[..., None] + jnp.einsum(
        "hmqk,khe->hmqe",
        weights.astype(jnp.bfloat16),
        values_in,
        preferred_element_type=jnp.float32,
    )
    return (new_max, run_total, summed)


def fold_keys(running, queries, keys_in, values_in, key_flags, bias_table, score_scale):
    full_blocks = keys_in.shape[0] // KEY_BLOCK
    if full_blocks > 1:
        edge = full_blocks * KEY_BLOCK
        stacked = (
            keys_in[:edge].reshape((full_blocks, KEY_BLOCK) + keys_in.shape[1:]),
            values_in[:edge].reshape((full_blocks, KEY_BLOCK) + values_in.shape[1:]),
        )
        if key_flags is not None:
            stacked = stacked + (key_flags[:edge].reshape(full_blocks, KEY_BLOCK),)

        def fold_step(current, block_data):
            flag_part = None if key_flags is None else block_data[2]
            return (
                fold_block(
                    current,
                    queries,
                    block_data[0],
                    block_data[1],
                    flag_part,
                    bias_table,
                    score_scale,
                ),
                None,
            )

        running, ignored = lax.scan(fold_step, running, stacked)
        keys_in = keys_in[edge:]
        values_in = values_in[edge:]
        key_flags = None if key_flags is None else key_flags[edge:]
    if keys_in.shape[0] > 0:
        running = fold_block(
            running, queries, keys_in, values_in, key_flags, bias_table, score_scale
        )
    return running


def body(
    latent,
    condition,
    context,
    context_vector,
    modulator,
    norm_gain,
    query_weight,
    key_weight,
    value_weight,
    head_gain,
    lambdas,
    context_bias,
    out_weight,
):
    model_width = latent.shape[2]
    local_heads = lambdas.shape[0]
    query_width = query_weight.shape[1]
    head_size = query_width // (2 * local_heads)
    value_size = value_weight.shape[1] // local_heads
    score_scale = head_size ** (-0.5)
    activated = jax.nn.silu(
        jnp.concatenate([condition, context_vector[None, :]], axis=0).astype(jnp.float32)
    )
    partial_terms = jnp.dot(
        activated.astype(jnp.bfloat16), modulator, preferred_element_type=jnp.float32
    )
    modulations = lax.psum(partial_terms, ("sp", "tp"))
    hidden = modulate(
        latent[0],
        norm_gain,
        modulations[0, :model_width],
        modulations[0, model_width : 2 * model_width],
    )
    ctx_hidden = modulate(
        context[0],
        norm_gain,
        modulations[1, :model_width],
        modulations[1, model_width : 2 * model_width],
    )
    gate_vector = modulations[0, 2 * model_width :]
    incoming = lax.all_gather(hidden, "tp", axis=0, tiled=True)
    projected = jnp.concatenate(
        [
            jnp.dot(incoming, query_weight, preferred_element_type=jnp.float32),
            jnp.dot(incoming, key_weight, preferred_element_type=jnp.float32),
            jnp.dot(incoming, value_weight, preferred_element_type=jnp.float32),
        ],
        axis=1,
    ).astype(jnp.bfloat16)
    query_rows = projected.shape[0]
    queries = projected[:, :query_width].reshape(query_rows, local_heads, 2, head_size)
    own_keys = projected[:, query_width : 2 * query_width]
    own_values = projected[:, 2 * query_width :]
    gathered_context = lax.all_gather(ctx_hidden, "sp", axis=0, tiled=True)
    ctx_keys = jnp.dot(gathered_context, key_weight, preferred_element_type=jnp.float32).astype(
        jnp.bfloat16
    )
    ctx_values = jnp.dot(gathered_context, value_weight, preferred_element_type=jnp.float32).astype(
        jnp.bfloat16
    )
    start_carry = (
        jnp.full((local_heads, 2, query_rows), LOW_START, jnp.float32),
        jnp.zeros((local_heads, 2, query_rows), jnp.float32),
        jnp.zeros((local_heads, 2, query_rows, value_size), jnp.float32),
    )
    pieces = (own_keys, own_values)
    initial = fold_keys(
        start_carry,
        queries,
        ctx_keys.reshape(-1, local_heads, 2, head_size),
        ctx_values.reshape(-1, local_heads, value_size),
        jnp.ones((ctx_keys.shape[0],), jnp.float32),
        context_bias,
        score_scale,
    )
    incoming = (
        lax.all_gather(pieces[0], "sp", axis=0, tiled=True),
        lax.all_gather(pieces[1], "sp", axis=0, tiled=True),
    )
    run_max, run_total, summed = fold_keys(
        initial,
        queries,
        incoming[0].reshape(-1, local_heads, 2, head_size),
        incoming[1].reshape(-1, local_heads, value_size),
        None,
        context_bias,
        score_scale,
    )
    mixed = (
        summed[:, 0] / run_total[:, 0, :, None]
        - lambdas[:, None, None] * summed[:, 1] / run_total[:, 1, :, None]
    )
    normed = (
        mixed
        * lax.rsqrt(jnp.mean(mixed * mixed, axis=-1, keepdims=True) + EPSILON)
        * head_gain
        * OUT_SCALE
    )
    attended = (
        jnp.transpose(normed, (1, 0, 2))
        .reshape(query_rows, local_heads * value_size)
        .astype(jnp.bfloat16)
    )
    exchanged = lax.all_to_all(attended, "tp", split_axis=0, concat_axis=1, tiled=True)
    whole_weight = lax.all_gather(out_weight, "tp", axis=0, tiled=True)
    branch = jnp.dot(exchanged, whole_weight, preferred_element_type=jnp.float32)
    result = (latent[0].astype(jnp.float32) + gate_vector * branch).astype(jnp.bfloat16)
    return result[None]


def solution(mesh):
    placed = (
        P("dp", ("sp", "tp"), None),
        P("dp", ("sp", "tp")),
        P("dp", "sp", None),
        P(("sp", "tp")),
        P(("sp", "tp"), None),
        P(),
        P(None, "tp"),
        P(None, "tp"),
        P(None, "tp"),
        P(),
        P("tp"),
        P("tp", None),
        P("tp", None),
    )
    return jax.shard_map(
        body, mesh=mesh, in_specs=placed, out_specs=P("dp", ("sp", "tp"), None), check_vma=False
    )
```

profile of v0, /device:TPU:0, one launch (start us, length us, event | category | flops | bytes accessed | tf_op | source)
XLA Modules:
  0.0 170.0 jit_solution(7644564545617815921)
XLA Ops:
  6.6 1.4 copy-done
  8.0 1.0 fusion.43
  9.0 78.7 %psum.7 = f32[2,6144]{1,0:T(2,128)S(1)} all-reduce(f32[2,6144]{1,0:T(2,128)S(1)} %fusion.43), channel_id=1, replica_groups=mesh['sp'=4,'tp'=4,'dp'=2] {'sp','tp'}, use_global_device_ids=true, to_apply=%region_0.1 | all-reduce | flops 12288 | bytes 98304 | tf_op jit(solution)/shard_map/psum | solution.py:103
  87.6 0.6 slice_add_fusion.1
  88.3 1.1 fusion.14
  89.4 1.6 fusion.18
  91.0 0.7 all-gather.5.cloned.1.call-update
  92.0 13.4 %all_gather.16 = bf16[32,2048]{1,0:T(8,128)(2,1)S(1)} all-gather(bf16[8,2048]{1,0:T(8,128)(2,1)S(1)} %fusion.27), channel_id=1, replica_groups=mesh['sp'=4,'tp'=4,'dp'=2] {'sp'}, dimensions={0}, use_global_device_ids=true | all-gather | bytes 163840 | tf_op jit(solution)/shard_map/all_gather | solution.py:130
  105.4 0.2 convolution_convert_fusion.4
  106.3 7.2 %all-gather.3.cloned.1.call-done = bf16[256,2048]{1,0:T(8,128)(2,1)} async-done(((bf16[64,2048]{1,0:T(8,128)(2,1)}), bf16[256,2048]{1,0:T(8,128)(2,1)}) %all-gather.3.cloned.1.call-update) | async-done | bytes 1048592 | tf_op jit(solution)/shard_map/all_gather | solution.py:117
  113.5 1.9 %convolution_convert_fusion.1 = bf16[256,128]{1,0:T(8,128)(2,1)S(1)} fusion(bf16[256,2048]{1,0:T(8,128)(2,1)} %all-gather.3.cloned.1.call-done, bf16[2048,128]{1,0:T(8,128)(2,1)} %param.20), kind=kOutput, calls=%fused_computation.13 | convolution fusion | flops 134250496 | bytes 1638400 | tf_op jit(solution)/shard_map/dot_general | solution.py:121
  115.4 14.6 %all_gather.17 = bf16[1024,128]{1,0:T(8,128)(2,1)} all-gather(bf16[256,128]{1,0:T(8,128)(2,1)S(1)} %convolution_convert_fusion.1), channel_id=1, replica_groups=mesh['sp'=4,'tp'=4,'dp'=2] {'sp'}, dimensions={0}, use_global_device_ids=true | all-gather | bytes 327680 | tf_op jit(solution)/shard_map/all_gather | solution.py:153
  130.0 1.8 %copy.30 = bf16[1024,128]{0,1:T(8,128)(2,1)} copy(bf16[1024,128]{1,0:T(8,128)(2,1)} %all_gather.17) | data formatting | bytes 524288 | tf_op jit(solution)/shard_map/all_gather | solution.py:153
  131.8 0.4 convolution_convert_fusion
  132.2 14.5 %all_gather.18 = bf16[1024,128]{1,0:T(8,128)(2,1)S(1)} all-gather(bf16[256,128]{1,0:T(8,128)(2,1)S(1)} %convolution_convert_fusion), channel_id=1, replica_groups=mesh['sp'=4,'tp'=4,'dp'=2] {'sp'}, dimensions={0}, use_global_device_ids=true | all-gather | bytes 327680 | tf_op jit(solution)/shard_map/all_gather | solution.py:154
  146.7 0.5 convolution_convert_fusion.2
  147.3 0.6 multiply_reduce_fusion
  147.9 1.3 copy-done.1
  149.2 0.5 fusion.10
  149.7 0.4 fusion.7
  150.2 2.1 %fusion.3 = f32[2,256]{1,0:T(2,128)S(1)} fusion(f32[2,256,1024]{2,1,0:T(8,128)} %copy-done.1, f32[2,256]{1,0:T(2,128)S(1)} %get-tuple-element.15), kind=kLoop, calls=%fused_computation.6 | loop fusion | flops 1572352 | bytes 2101248 | tf_op jit(solution)/shard_map/reduce_sum | solution.py:29
  152.3 0.2 fusion.22
  153.0 7.4 %all_to_all.16 = bf16[4,64,128]{2,1,0:T(8,128)(2,1)S(1)} all-to-all(bf16[4,64,128]{2,1,0:T(8,128)(2,1)S(1)} %multiply_convert_fusion), channel_id=1, replica_groups=mesh['sp'=4,'tp'=4,'dp'=2] {'tp'}, dimensions={0} | all-to-all | bytes 131072 | tf_op jit(solution)/shard_map/all_to_all | solution.py:180
  160.4 2.8 %fusion.2 = bf16[1,64,2048]{2,1,0:T(8,128)(2,1)} fusion(bf16[512,2048]{1,0:T(8,128)(2,1)} %all-gather.5.cloned.1.call-done, bf16[1,64,2048]{2,1,0:T(8,128)(2,1)S(1)} %copy-done.3, f32[2048]{0:T(1024)S(1)} %bitcast.94, bf16[4,64,128]{2,1,0:T(8,128)(2,1)S(1)} %all_to_all.16), kind=kOutput, calls=%fused_computation.3 | convolution fusion | flops 134742016 | bytes 2695168 | tf_op jit(solution)/shard_map/dot_general | solution.py:182
  (44 shorter events, 1.1 us)
Async XLA Ops:
  6.5 1.4 copy-start
  6.5 82.8 %copy-start.3 = (bf16[1,64,2048]{2,1,0:T(8,128)(2,1)S(1)}, bf16[1,64,2048]{2,1,0:T(8,128)(2,1)}, u32[]{:S(2)}) copy-start(bf16[1,64,2048]{2,1,0:T(8,128)(2,1)} %param.13) | copy-start | bytes 786436
  6.5 85.4 %copy-start.10 = (f32[2048]{0:T(1024)S(1)}, f32[2048]{0:T(1024)}, u32[]{:S(2)}) copy-start(f32[2048]{0:T(1024)} %param.18) | copy-start | bytes 24580
  6.5 85.2 %copy-start.8 = (bf16[1,8,2048]{2,1,0:T(8,128)(2,1)S(1)}, bf16[1,8,2048]{2,1,0:T(8,128)(2,1)}, u32[]{:S(2)}) copy-start(bf16[1,8,2048]{2,1,0:T(8,128)(2,1)} %param.15) | copy-start | bytes 98308
  6.5 98.8 %copy-start.5 = (bf16[2048,128]{1,0:T(8,128)(2,1)S(1)}, bf16[2048,128]{1,0:T(8,128)(2,1)}, u32[]{:S(2)}) copy-start(bf16[2048,128]{1,0:T(8,128)(2,1)} %param.20) | copy-start | bytes 1572868
  6.6 107.0 %all-gather.3.cloned.1.call-start = ((), (), s32[]{:S(2)}) async-start(), calls=%async_computation.1 | async-start | bytes 1310720 | tf_op jit(solution)/shard_map/all_gather | solution.py:117
  91.0 40.8 %copy-start.4 = (bf16[2048,128]{1,0:T(8,128)(2,1)S(1)}, bf16[2048,128]{1,0:T(8,128)(2,1)}, u32[]{:S(2)}) copy-start(bf16[2048,128]{1,0:T(8,128)(2,1)} %param.21) | copy-start | bytes 1572868
  91.0 69.4 %all-gather.5.cloned.1.call-start = ((), (), s32[]{:S(2)}) async-start(), calls=%async_computation.2 | async-start | bytes 2621440 | tf_op jit(solution)/shard_map/all_gather | solution.py:181
  113.5 18.3 %copy-start.2 = (bf16[256,2048]{1,0:T(8,128)(2,1)S(1)}, bf16[256,2048]{1,0:T(8,128)(2,1)}, u32[]{:S(2)}) copy-start(bf16[256,2048]{1,0:T(8,128)(2,1)} %all-gather.3.cloned.1.call-done) | copy-start | bytes 3145732
  131.8 14.9 %copy-start.7 = (bf16[2048,128]{1,0:T(8,128)(2,1)S(1)}, bf16[2048,128]{1,0:T(8,128)(2,1)}, u32[]{:S(2)}) copy-start(bf16[2048,128]{1,0:T(8,128)(2,1)} %param.19) | copy-start | bytes 1572868
  131.8 15.4 %copy-start.11 = (f32[1,2]{1,0:T(1,128)S(1)}, f32[1,2]{1,0:T(1,128)}, u32[]{:S(2)}) copy-start(f32[1,2]{1,0:T(1,128)} %param.24) | copy-start | bytes 28
  131.8 15.6 %copy-start.6 = (bf16[1024,128]{0,1:T(8,128)(2,1)S(1)}, bf16[1024,128]{0,1:T(8,128)(2,1)}, u32[]{:S(2)}) copy-start(bf16[1024,128]{0,1:T(8,128)(2,1)} %copy.30) | copy-start | bytes 786436
  147.9 1.3 copy-start.1
  149.7 3.1 %copy-start.12 = (f32[128]{0:T(128)S(1)}, f32[128]{0:T(128)}, u32[]{:S(2)}) copy-start(f32[128]{0:T(128)} %param.22) | copy-start | bytes 1540
  149.7 10.6 %copy-start.9 = (f32[1,2048]{1,0:T(1,128)S(1)}, f32[1,2048]{1,0:T(1,128)}, u32[]{:S(2)}) copy-start(f32[1,2048]{1,0:T(1,128)} %get-tuple-element.13) | copy-start | bytes 24580
Sparse Core Ops, SparseCore 0:
  91.1 22.3 all-gather.2
  115.3 35.1 all-gather.4
where the time goes:
time: 170 us
  blocking collectives  129 us (76%)
  between operations  14.3 us (8%)
  matrix products  8.34 us (5%)
  waiting for transfers between devices  7.88 us (5%)
  other arithmetic  6.08 us (4%)
  local copies, waits for them, and re-layouts  4.84 us (3%)
    psum x1, blocking collectives, body(): modulations = lax.psum(partial_terms, ('sp', 'tp'))  78.7 us
    all_gather x1, blocking collectives, body(): lax.all_gather(pieces[0], 'sp', axis=0, tiled=True)  14.6 us
    all_gather x1, blocking collectives, body(): lax.all_gather(pieces[1], 'sp', axis=0, tiled=True)  14.5 us
    all_gather x1, blocking collectives, body(): gathered_context = lax.all_gather(ctx_hidden, 'sp', axis=0, tiled=True)  13.4 us
    all_to_all x1, blocking collectives, body(): lax.all_to_all(attended, 'tp', split_axis=0, concat_axis=1, tiled=True)  7.38 us
    all_gather x1, waiting for transfers between devices, body(): incoming = lax.all_gather(hidden, 'tp', axis=0, tiled=True)  7.17 us
  transfers between devices with their start and end apart: 2, of which 1 were waited for; matrix products, arithmetic and copies ran while one was open for 6% of the time, Pallas kernels for 0%

commit v1 on v0

--- a/solution.py
+++ b/solution.py
@@ -100,7 +100,7 @@
     partial_terms = jnp.dot(
         activated.astype(jnp.bfloat16), modulator, preferred_element_type=jnp.float32
     )
-    modulations = lax.psum(partial_terms, ("sp", "tp"))
+    modulations = jnp.sum(lax.all_gather(partial_terms, ("sp", "tp")), axis=0)
     hidden = modulate(
         latent[0],
         norm_gain,

time: 170 us -> 138 us (0.81)
  blocking collectives: 129 us -> 97.1 us
    psum x1 -> x0, blocking collectives: 78.7 us -> none  [body(): modulations = lax.psum(partial_terms, ('sp', 'tp'))]
    all_gather x0 -> x1, blocking collectives: none -> 47.2 us  [body(): modulations = jnp.sum(lax.all_gather(partial_terms, ('sp', 'tp')), axis=0)]
  transfers between devices with their start and end apart: 2 -> 2, of which waited for: 1 -> 1; matrix products, arithmetic and copies ran while one was open for 6% -> 7% of each run, Pallas kernels for 0% -> 0%
where the time goes in v1:
time: 138 us; the launch traced here: 137 us
  blocking collectives  97.1 us (70%)
  between operations  14.2 us (10%)
  matrix products  8.34 us (6%)
  waiting for transfers between devices  7.88 us (6%)
  local copies, waits for them, and re-layouts  4.87 us (4%)
  other arithmetic  4.69 us (3%)
    all_gather x1, blocking collectives, body(): modulations = jnp.sum(lax.all_gather(partial_terms, ('sp', 'tp')), axis=0)  47.2 us
    all_gather x1, blocking collectives, body(): lax.all_gather(pieces[0], 'sp', axis=0, tiled=True)  14.6 us
    all_gather x1, blocking collectives, body(): lax.all_gather(pieces[1], 'sp', axis=0, tiled=True)  14.4 us
    all_gather x1, blocking collectives, body(): gathered_context = lax.all_gather(ctx_hidden, 'sp', axis=0, tiled=True)  13.4 us
    all_to_all x1, blocking collectives, body(): lax.all_to_all(attended, 'tp', split_axis=0, concat_axis=1, tiled=True)  7.41 us
    all_gather x1, waiting for transfers between devices, body(): incoming = lax.all_gather(hidden, 'tp', axis=0, tiled=True)  7.17 us
    dot_general x1, matrix products, body(): jnp.dot(exchanged, whole_weight, preferred_element_type=jnp.float32)  2.78 us
  transfers between devices with their start and end apart: 2, of which 1 were waited for; matrix products, arithmetic and copies ran while one was open for 7% of the time, Pallas kernels for 0%

profile of v1, /device:TPU:0, one launch (start us, length us, event | category | flops | bytes accessed | tf_op | source)
XLA Modules:
  0.0 137.1 jit_solution(15674720366132445127)
XLA Ops:
  6.5 1.4 %copy-done = bf16[128,6144]{1,0:T(8,128)(2,1)S(1)} copy-done((bf16[128,6144]{1,0:T(8,128)(2,1)S(1)}, bf16[128,6144]{1,0:T(8,128)(2,1)}, u32[]{:S(2)}) %copy-start) | copy-done | bytes 1572888
  7.9 1.0 convolution_bitcast_fusion
  9.0 47.2 %all-gather.1 = f32[16,2,6144]{2,1,0:T(2,128)S(1)} all-gather(f32[1,2,6144]{2,1,0:T(2,128)S(1)} %convolution_bitcast_fusion), channel_id=2, replica_groups=mesh['sp'=4,'tp'=4,'dp'=2] {'sp','tp'}, dimensions={0}, use_global_device_ids=true | all-gather | bytes 835584 | tf_op jit(solution)/shard_map/all_gather | solution.py:103
  56.2 0.3 reduce_sum.58
  56.4 0.6 slice_add_fusion.1
  57.2 0.9 fusion.18
  58.2 0.7 all-gather.7.cloned.1.call-update
  59.1 13.4 %all_gather.24 = bf16[32,2048]{1,0:T(8,128)(2,1)S(1)} all-gather(bf16[8,2048]{1,0:T(8,128)(2,1)S(1)} %fusion.27), channel_id=1, replica_groups=mesh['sp'=4,'tp'=4,'dp'=2] {'sp'}, dimensions={0}, use_global_device_ids=true | all-gather | bytes 163840 | tf_op jit(solution)/shard_map/all_gather | solution.py:130
  72.5 0.2 convolution_convert_fusion.4
  73.5 7.2 %all-gather.5.cloned.1.call-done = bf16[256,2048]{1,0:T(8,128)(2,1)} async-done(((bf16[64,2048]{1,0:T(8,128)(2,1)}), bf16[256,2048]{1,0:T(8,128)(2,1)}) %all-gather.5.cloned.1.call-update) | async-done | bytes 1048592 | tf_op jit(solution)/shard_map/all_gather | solution.py:117
  80.7 1.9 %convolution_convert_fusion.1 = bf16[256,128]{1,0:T(8,128)(2,1)S(1)} fusion(bf16[256,2048]{1,0:T(8,128)(2,1)} %all-gather.5.cloned.1.call-done, bf16[2048,128]{1,0:T(8,128)(2,1)} %param.20), kind=kOutput, calls=%fused_computation.14 | convolution fusion | flops 134250496 | bytes 1638400 | tf_op jit(solution)/shard_map/dot_general | solution.py:121
  82.5 14.6 %all_gather.25 = bf16[1024,128]{1,0:T(8,128)(2,1)} all-gather(bf16[256,128]{1,0:T(8,128)(2,1)S(1)} %convolution_convert_fusion.1), channel_id=1, replica_groups=mesh['sp'=4,'tp'=4,'dp'=2] {'sp'}, dimensions={0}, use_global_device_ids=true | all-gather | bytes 327680 | tf_op jit(solution)/shard_map/all_gather | solution.py:153
  97.1 1.8 %copy.30 = bf16[1024,128]{0,1:T(8,128)(2,1)} copy(bf16[1024,128]{1,0:T(8,128)(2,1)} %all_gather.25) | data formatting | bytes 524288 | tf_op jit(solution)/shard_map/all_gather | solution.py:153
  98.9 0.4 convolution_convert_fusion
  99.4 14.4 %all_gather.26 = bf16[1024,128]{1,0:T(8,128)(2,1)S(1)} all-gather(bf16[256,128]{1,0:T(8,128)(2,1)S(1)} %convolution_convert_fusion), channel_id=1, replica_groups=mesh['sp'=4,'tp'=4,'dp'=2] {'sp'}, dimensions={0}, use_global_device_ids=true | all-gather | bytes 327680 | tf_op jit(solution)/shard_map/all_gather | solution.py:154
  113.8 0.5 convolution_convert_fusion.2
  114.5 0.6 multiply_reduce_fusion
  115.0 1.3 copy-done.1
  116.3 0.5 fusion.10
  116.9 0.4 fusion.7
  117.3 2.1 %fusion.3 = f32[2,256]{1,0:T(2,128)S(1)} fusion(f32[2,256,1024]{2,1,0:T(8,128)} %copy-done.1, f32[2,256]{1,0:T(2,128)S(1)} %get-tuple-element.15), kind=kLoop, calls=%fused_computation.7 | loop fusion | flops 1572352 | bytes 2101248 | tf_op jit(solution)/shard_map/reduce_sum | solution.py:29
  119.4 0.2 fusion.22
  120.1 7.4 %all_to_all.16 = bf16[4,64,128]{2,1,0:T(8,128)(2,1)S(1)} all-to-all(bf16[4,64,128]{2,1,0:T(8,128)(2,1)S(1)} %multiply_convert_fusion), channel_id=1, replica_groups=mesh['sp'=4,'tp'=4,'dp'=2] {'tp'}, dimensions={0} | all-to-all | bytes 131072 | tf_op jit(solution)/shard_map/all_to_all | solution.py:180
  127.5 2.8 %fusion.2 = bf16[1,64,2048]{2,1,0:T(8,128)(2,1)} fusion(bf16[512,2048]{1,0:T(8,128)(2,1)} %all-gather.7.cloned.1.call-done, bf16[1,64,2048]{2,1,0:T(8,128)(2,1)S(1)} %copy-done.3, f32[2048]{0:T(1024)S(1)} %bitcast.96, bf16[4,64,128]{2,1,0:T(8,128)(2,1)S(1)} %all_to_all.16), kind=kOutput, calls=%fused_computation.4 | convolution fusion | flops 134742016 | bytes 2695168 | tf_op jit(solution)/shard_map/dot_general | solution.py:182
  (45 shorter events, 1.3 us)
Async XLA Ops:
  6.5 1.4 %copy-start = (bf16[128,6144]{1,0:T(8,128)(2,1)S(1)}, bf16[128,6144]{1,0:T(8,128)(2,1)}, u32[]{:S(2)}) copy-start(bf16[128,6144]{1,0:T(8,128)(2,1)} %param.17) | copy-start | bytes 4718596
  6.5 50.5 %copy-start.3 = (bf16[1,64,2048]{2,1,0:T(8,128)(2,1)S(1)}, bf16[1,64,2048]{2,1,0:T(8,128)(2,1)}, u32[]{:S(2)}) copy-start(bf16[1,64,2048]{2,1,0:T(8,128)(2,1)} %param.13) | copy-start | bytes 786436
  6.5 50.7 %copy-start.10 = (f32[2048]{0:T(1024)S(1)}, f32[2048]{0:T(1024)}, u32[]{:S(2)}) copy-start(f32[2048]{0:T(1024)} %param.18) | copy-start | bytes 24580
  6.5 74.1 %all-gather.5.cloned.1.call-start = ((), (), s32[]{:S(2)}) async-start(), calls=%async_computation.1 | async-start | bytes 1310720 | tf_op jit(solution)/shard_map/all_gather | solution.py:117
  7.9 51.0 %copy-start.8 = (bf16[1,8,2048]{2,1,0:T(8,128)(2,1)S(1)}, bf16[1,8,2048]{2,1,0:T(8,128)(2,1)}, u32[]{:S(2)}) copy-start(bf16[1,8,2048]{2,1,0:T(8,128)(2,1)} %param.15) | copy-start | bytes 98308
  8.9 63.6 %copy-start.5 = (bf16[2048,128]{1,0:T(8,128)(2,1)S(1)}, bf16[2048,128]{1,0:T(8,128)(2,1)}, u32[]{:S(2)}) copy-start(bf16[2048,128]{1,0:T(8,128)(2,1)} %param.20) | copy-start | bytes 1572868
  58.1 40.8 %copy-start.4 = (bf16[2048,128]{1,0:T(8,128)(2,1)S(1)}, bf16[2048,128]{1,0:T(8,128)(2,1)}, u32[]{:S(2)}) copy-start(bf16[2048,128]{1,0:T(8,128)(2,1)} %param.21) | copy-start | bytes 1572868
  58.1 69.4 %all-gather.7.cloned.1.call-start = ((), (), s32[]{:S(2)}) async-start(), calls=%async_computation.2 | async-start | bytes 2621440 | tf_op jit(solution)/shard_map/all_gather | solution.py:181
  80.7 18.3 %copy-start.2 = (bf16[256,2048]{1,0:T(8,128)(2,1)S(1)}, bf16[256,2048]{1,0:T(8,128)(2,1)}, u32[]{:S(2)}) copy-start(bf16[256,2048]{1,0:T(8,128)(2,1)} %all-gather.5.cloned.1.call-done) | copy-start | bytes 3145732
  98.9 14.9 %copy-start.7 = (bf16[2048,128]{1,0:T(8,128)(2,1)S(1)}, bf16[2048,128]{1,0:T(8,128)(2,1)}, u32[]{:S(2)}) copy-start(bf16[2048,128]{1,0:T(8,128)(2,1)} %param.19) | copy-start | bytes 1572868
  98.9 15.4 %copy-start.11 = (f32[1,2]{1,0:T(1,128)S(1)}, f32[1,2]{1,0:T(1,128)}, u32[]{:S(2)}) copy-start(f32[1,2]{1,0:T(1,128)} %param.24) | copy-start | bytes 28
  98.9 15.5 %copy-start.6 = (bf16[1024,128]{0,1:T(8,128)(2,1)S(1)}, bf16[1024,128]{0,1:T(8,128)(2,1)}, u32[]{:S(2)}) copy-start(bf16[1024,128]{0,1:T(8,128)(2,1)} %copy.30) | copy-start | bytes 786436
  115.0 1.3 copy-start.1
  116.9 3.1 %copy-start.12 = (f32[128]{0:T(128)S(1)}, f32[128]{0:T(128)}, u32[]{:S(2)}) copy-start(f32[128]{0:T(128)} %param.22) | copy-start | bytes 1540
  116.9 10.7 %copy-start.9 = (f32[1,2048]{1,0:T(1,128)S(1)}, f32[1,2048]{1,0:T(1,128)}, u32[]{:S(2)}) copy-start(f32[1,2048]{1,0:T(1,128)} %get-tuple-element.13) | copy-start | bytes 24580
Sparse Core Ops, SparseCore 0:
  58.3 22.3 all-gather.4
  82.5 35.1 all-gather.6
